TPU v7x, 32 devices: a whole 2x2x4 slice. The times are simulated.
32 devices in a mesh: sp: 8 (over z, y), dp: 4 (over x, core).
Axes of the slice: x: 2, y: 2, z: 4, core: 2. Of those that a mesh axis runs over, the one named last changes fastest.
Arguments:
- residual_input: bfloat16 [4, 1024, 2048], P('dp', 'sp'), may hold values from -6 to 6
- queries: bfloat16 [4, 1024, 512], P('dp', 'sp'), may hold values from -6 to 6
- keys: bfloat16 [4, 1024, 512], P('dp', 'sp'), may hold values from -6 to 6
- values: bfloat16 [4, 1024, 1024], P('dp', 'sp'), may hold values from -6 to 6
- gate_logits: bfloat16 [4, 1024, 32], P('dp', 'sp'), may hold values from -6 to 6
- retention_offset: float32 [8, 2], P('sp'), may hold values from 3 to 12
- log_forget_extra: float32 [4, 8, 1024], P('dp', 'sp'), may hold values from -2.76 to 0
- lane_amplifier: float32 [1024], P('sp'), may hold values from 0.1 to 1.9
- output_gate_logits: bfloat16 [4, 1024, 1024], P('dp', 'sp'), may hold values from -6 to 6
- output_projection: bfloat16 [1024, 2048], P(None, 'dp'), may hold values from -0.1875 to 0.1875
- cell_norm_gain: float32 [2048], replicated, may hold values from 0.1 to 1.9
- expert_norm_gain: float32 [2048], replicated, may hold values from 0.1 to 1.9
- expert_index: int32 [4, 1024, 2], P('dp', 'sp'), may hold values from 0 to 31, all different within a row; in each aligned block of 128 rows (0 to 127, 128 to 255, ..., all dimensions but the last counted through in order) at most 16 rows name the same one
- group_mixing_weight: float32 [4, 1024, 4], P('dp', 'sp'), may hold values from 0.05 to 1
- within_group_weight: float32 [4, 1024, 2], P('dp', 'sp'), may hold values from 0.1 to 1
- gate_weight: bfloat16 [32, 2048, 1024], P(('sp', 'dp')), may hold values from -0.125 to 0.125
- up_weight: bfloat16 [32, 2048, 1024], P(('sp', 'dp')), may hold values from -0.125 to 0.125
- down_weight: bfloat16 [32, 1024, 2048], P(('sp', 'dp')), may hold values from -0.75 to 0.75
Outputs:
- stream_out: bfloat16 [4, 1024, 2048], P('dp', 'sp')
Inputs may be any that keep to these rules, and one draw needn't show every extreme that they name: `expert_index`: A token's two experts differ; among the 128 tokens of one device no expert is named more than 16 times, a bound that some block reaches.
All inputs are finite; a program needn't handle non-finite values.
Results may differ from a plain program's by a relative error of at most 0.0095.
Values may be sent and summed in bfloat16 or wider, within the bound.
A program may use at most 128 MiB of HBM per device.

v0:
```python
from functools import partial

import jax
import jax.numpy as jnp
from jax import lax
from jax.sharding import PartitionSpec as P

SPAN_STEPS = 512


EPS = 1e-06
HIGH_PRECISION = lax.Precision.HIGHEST


def block_states(keys_f, values_f, in_gate, log_forget, span_steps):
    length, key_width = keys_f.shape
    blocks = length // span_steps
    blocked_keys = keys_f.reshape(blocks, span_steps, key_width)
    blocked_values = values_f.reshape(blocks, span_steps, values_f.shape[1])
    running = jnp.cumsum(log_forget.reshape(blocks, span_steps), axis=1)
    block_end = running[:, -1]
    weight_log = block_end[:, None] - running + in_gate.reshape(blocks, span_steps)
    local_top = jnp.max(weight_log, axis=1)
    weight_table = jnp.exp(weight_log - local_top[:, None])
    local_memory = jnp.einsum(
        "ryd,rya->rda",
        blocked_values * weight_table[:, :, None],
        blocked_keys,
        precision=HIGH_PRECISION,
    )
    local_normalizer = jnp.einsum(
        "nb,nby->ny", weight_table, blocked_keys, precision=HIGH_PRECISION
    )

    def advance(carried_state, inputs):
        memory, normal, stable = carried_state
        end_log, top_log, memory_new, normal_new = inputs
        raised = jnp.maximum(end_log + stable, top_log)
        keep_old = jnp.exp(end_log + stable - raised)
        keep_new = jnp.exp(top_log - raised)
        updated = (
            keep_old * memory + keep_new * memory_new,
            keep_old * normal + keep_new * normal_new,
            raised,
        )
        return (updated, (memory, normal, stable))

    initial = (
        jnp.zeros((values_f.shape[1], key_width), jnp.float32),
        jnp.zeros((key_width,), jnp.float32),
        jnp.zeros((), jnp.float32),
    )
    _, entries = lax.scan(advance, initial, (block_end, local_top, local_memory, local_normalizer))
    return entries


def direction_out(query_f, keys_f, values_f, in_gate, log_forget, span_steps):
    entry_memory, entry_normal, entry_top = block_states(
        keys_f, values_f, in_gate, log_forget, span_steps
    )
    length, key_width = keys_f.shape
    blocks = length // span_steps
    query_blocks = query_f.reshape(blocks, span_steps, key_width) * key_width ** (-0.5)
    blocked_keys = keys_f.reshape(blocks, span_steps, key_width)
    blocked_values = values_f.reshape(blocks, span_steps, values_f.shape[1])
    running = jnp.cumsum(log_forget.reshape(blocks, span_steps), axis=1)
    entry_log = running + entry_top[:, None]
    pair_log = (
        running[:, :, None] - running[:, None, :] + in_gate.reshape(blocks, span_steps)[:, None, :]
    )
    earlier = jnp.tril(jnp.ones((span_steps, span_steps), dtype=bool))
    pair_log = jnp.where(earlier[None], pair_log, -jnp.inf)
    top_log = jnp.maximum(entry_log, jnp.max(pair_log, axis=2))
    scores = jnp.einsum(
        "ctk,csk->cts", query_blocks, blocked_keys, precision=HIGH_PRECISION
    ) * jnp.exp(pair_log - top_log[:, :, None])
    carried = jnp.exp(entry_log - top_log)
    numerator = carried[:, :, None] * jnp.einsum(
        "cvk,ctk->ctv", entry_memory, query_blocks, precision=HIGH_PRECISION
    )
    numerator = numerator + jnp.einsum(
        "cts,csv->ctv", scores, blocked_values, precision=HIGH_PRECISION
    )
    denominator = carried * jnp.einsum(
        "ck,ctk->ct", entry_normal, query_blocks, precision=HIGH_PRECISION
    ) + jnp.sum(scores, axis=2)
    output = numerator / jnp.maximum(jnp.abs(denominator), jnp.exp(-top_log))[:, :, None]
    return output.reshape(length, blocked_values.shape[2])


def lane_blend(
    lane_question,
    lane_addresses,
    lane_contents,
    lane_switches,
    lane_offset,
    lane_spread,
    lane_rescaling,
    span_steps,
):
    query_f = lane_question.astype(jnp.float32)
    keys_f = lane_addresses.astype(jnp.float32)
    values_f = lane_contents.astype(jnp.float32)
    retention_entries = lane_switches.astype(jnp.float32)
    onward_fading = jax.nn.log_sigmoid(retention_entries[:, 1] + lane_offset[0]) + lane_spread
    reverse_fading = jax.nn.log_sigmoid(retention_entries[:, 3] + lane_offset[1]) + lane_spread
    forward = direction_out(
        query_f, keys_f, values_f, retention_entries[:, 0], onward_fading, span_steps
    )
    backward = direction_out(
        query_f[::-1],
        keys_f[::-1],
        values_f[::-1],
        retention_entries[::-1, 2],
        reverse_fading[::-1],
        span_steps,
    )[::-1]
    total = forward + backward
    normed = (
        total * lax.rsqrt(jnp.mean(total * total, axis=1, keepdims=True) + EPS) * lane_rescaling
    )
    return normed.astype(jnp.bfloat16)


def on_device(
    residual_input,
    queries,
    keys,
    values,
    gate_logits,
    retention_offset,
    log_forget_extra,
    lane_amplifier,
    output_gate_logits,
    output_projection,
    cell_norm_gain,
    expert_norm_gain,
    expert_index,
    group_mixing_weight,
    within_group_weight,
    gate_weight,
    up_weight,
    down_weight,
):
    query_all, keys_all, values_all, gates_all = (
        lax.all_to_all(queries, "sp", split_axis=2, concat_axis=1, tiled=True),
        lax.all_to_all(keys, "sp", split_axis=2, concat_axis=1, tiled=True),
        lax.all_to_all(values, "sp", split_axis=2, concat_axis=1, tiled=True),
        lax.all_to_all(gate_logits, "sp", split_axis=2, concat_axis=1, tiled=True),
    )
    length = query_all.shape[1]
    per_dev = retention_offset.shape[0]
    key_width = query_all.shape[2] // per_dev
    value_width = values_all.shape[2] // per_dev

    def split_heads(array, width):
        return array.reshape(length, per_dev, width).transpose(1, 0, 2)

    mixed_heads = jax.vmap(partial(lane_blend, span_steps=SPAN_STEPS))(
        split_heads(query_all, key_width),
        split_heads(keys_all, key_width),
        split_heads(values_all, value_width),
        split_heads(gates_all, 4),
        retention_offset,
        log_forget_extra[0],
        lane_amplifier.reshape(per_dev, value_width),
    )
    mixed_local = mixed_heads.transpose(1, 0, 2).reshape(1, length, per_dev * value_width)
    mixed_output = lax.all_to_all(mixed_local, "sp", split_axis=1, concat_axis=2, tiled=True)
    tok_rows = mixed_output.shape[1]
    width = residual_input.shape[2]
    gated = (
        mixed_output.astype(jnp.float32) * jax.nn.sigmoid(output_gate_logits.astype(jnp.float32))
    ).astype(jnp.bfloat16)
    gated = gated.reshape(tok_rows, gated.shape[2])
    proj = jnp.dot(
        gated,
        lax.all_gather(output_projection, "dp", axis=1, tiled=True),
        preferred_element_type=jnp.float32,
    )
    stream_f = residual_input.reshape(tok_rows, width).astype(jnp.float32)
    stream = (
        stream_f
        + cell_norm_gain * proj * lax.rsqrt(jnp.mean(proj * proj, axis=1, keepdims=True) + EPS)
    ).astype(jnp.bfloat16)
    stream_f = stream.astype(jnp.float32)
    moe_in = (
        expert_norm_gain
        * stream_f
        * lax.rsqrt(jnp.mean(stream_f * stream_f, axis=1, keepdims=True) + EPS)
    ).astype(jnp.bfloat16)
    seq_devices = lax.axis_size("sp")
    seq_groups = lax.axis_size("dp")
    experts = seq_devices * seq_groups
    capacity = 4 * tok_rows // experts
    flat_ids = expert_index.reshape(tok_rows * 2)
    onehot = (flat_ids[:, None] == jnp.arange(experts, dtype=jnp.int32)[None, :]).astype(jnp.int32)
    slot_index = jnp.sum((jnp.cumsum(onehot, axis=0) - onehot) * onehot, axis=1)
    target = flat_ids * capacity + slot_index
    slot_table = (
        target[:, None] == jnp.arange(experts * capacity, dtype=jnp.int32)[None, :]
    ).astype(jnp.bfloat16)
    token_table = jnp.sum(slot_table.reshape(tok_rows, 2, experts * capacity), axis=1)
    outgoing = lax.dot_general(
        token_table, moe_in, (((0,), (0,)), ((), ())), preferred_element_type=jnp.float32
    ).astype(jnp.bfloat16)
    incoming = lax.all_to_all(outgoing, ("sp", "dp"), split_axis=0, concat_axis=0, tiled=True)
    hidden = (
        jax.nn.silu(jnp.dot(incoming, gate_weight[0], preferred_element_type=jnp.float32))
        * jnp.dot(incoming, up_weight[0], preferred_element_type=jnp.float32)
    ).astype(jnp.bfloat16)
    produced = jnp.dot(hidden, down_weight[0], preferred_element_type=jnp.float32).astype(
        jnp.bfloat16
    )
    returned = lax.all_to_all(produced, ("sp", "dp"), split_axis=0, concat_axis=0, tiled=True)
    group_count = group_mixing_weight.shape[2]
    group_of = expert_index.reshape(tok_rows, 2) // (experts // group_count)
    group_hit = (
        group_of[:, :, None] == jnp.arange(group_count, dtype=jnp.int32)[None, None, :]
    ).astype(jnp.float32)
    chosen_group = jnp.sum(
        group_mixing_weight.reshape(tok_rows, 1, group_count) * group_hit, axis=2
    )
    route = chosen_group * within_group_weight.reshape(tok_rows, 2)
    picked = jnp.dot(slot_table, returned, preferred_element_type=jnp.float32).reshape(
        tok_rows, 2, width
    )
    mixture = jnp.sum(picked * route[:, :, None], axis=1)
    return (stream_f + mixture).astype(jnp.bfloat16).reshape(1, tok_rows, width)


def solution(mesh):
    in_specs = (
        P("dp", "sp", None),
        P("dp", "sp", None),
        P("dp", "sp", None),
        P("dp", "sp", None),
        P("dp", "sp", None),
        P("sp", None),
        P("dp", "sp", None),
        P("sp"),
        P("dp", "sp", None),
        P(None, "dp"),
        P(),
        P(),
        P("dp", "sp", None),
        P("dp", "sp", None),
        P("dp", "sp", None),
        P(("sp", "dp"), None, None),
        P(("sp", "dp"), None, None),
        P(("sp", "dp"), None, None),
    )
    out_specs = P("dp", "sp", None)
    return jax.shard_map(
        on_device, mesh=mesh, in_specs=in_specs, out_specs=out_specs, check_vma=False
    )
```

profile of v0, /device:TPU:0, one launch (start us, length us, event | category | flops | bytes accessed | tf_op | source)
XLA Modules:
  0.0 241.5 jit_solution(5375349144987447761)
XLA Ops:
  9.1 7.3 %all-to-all-start = ((bf16[8,2,256]{2,1,0:T(2,128)(2,1)}), bf16[8,2,256]{2,1,0:T(2,128)(2,1)S(1)}, u32[]{:S(2)}, u32[]{:S(2)}) async-start(bf16[8,2,256]{2,1,0:T(2,128)(2,1)} %reshape.1268), calls=%async_computation | async-start | bytes 16384 | tf_op jit(solution)/shard_map/all_to_all | solution.py:149
  24.1 2.2 reduce.38
  29.8 6.0 %all-to-all-start.2 = ((bf16[8,2,4096]{2,1,0:T(2,128)(2,1)}), bf16[8,2,4096]{2,1,0:T(2,128)(2,1)S(1)}, u32[]{:S(2)}, u32[]{:S(2)}) async-start(bf16[8,2,4096]{2,1,0:T(2,128)(2,1)} %reshape.1266), calls=%async_computation.2 | async-start | bytes 262144 | tf_op jit(solution)/shard_map/all_to_all | solution.py:147
  43.1 5.8 %all-to-all-start.3 = ((bf16[8,2,4096]{2,1,0:T(2,128)(2,1)}), bf16[8,2,4096]{2,1,0:T(2,128)(2,1)S(1)}, u32[]{:S(2)}, u32[]{:S(2)}) async-start(bf16[8,2,4096]{2,1,0:T(2,128)(2,1)} %reshape.1270), calls=%async_computation.3 | async-start | bytes 262144 | tf_op jit(solution)/shard_map/all_to_all | solution.py:146
  50.4 5.8 %all-to-all-done.3 = bf16[8,2,4096]{2,1,0:T(2,128)(2,1)S(1)} async-done(((bf16[8,2,4096]{2,1,0:T(2,128)(2,1)}), bf16[8,2,4096]{2,1,0:T(2,128)(2,1)S(1)}, u32[]{:S(2)}, u32[]{:S(2)}) %all-to-all-start.3) | async-done | bytes 131104 | tf_op jit(solution)/shard_map/all_to_all | solution.py:146
  56.3 3.6 %all-to-all-start.1 = ((bf16[8,2,8192]{2,1,0:T(2,128)(2,1)}), bf16[8,2,8192]{2,1,0:T(2,128)(2,1)S(1)}, u32[]{:S(2)}, u32[]{:S(2)}) async-start(bf16[8,2,8192]{2,1,0:T(2,128)(2,1)} %reshape.1264), calls=%async_computation.1 | async-start | bytes 524288 | tf_op jit(solution)/shard_map/all_to_all | solution.py:148
  60.1 1.7 rev.21
  62.0 1.7 rev.22
  65.8 2.0 all-to-all-done.1
  69.0 5.8 %while.42 = (s32[]{:T(128)}, f32[1,128,64]{2,1,0:T(8,128)S(1)}, f32[1,64]{1,0:T(1,128)S(1)}, f32[1]{0:T(128)}, f32[2,1,128,64]{3,2,1,0:T(8,128)S(1)}, /*index=5*...) while((s32[]{:T(128)}, f32[1,128,64]{2,1,0:T(8,128)S(1)}, ...), condition=%wide.region_4.5_spmd.clone, body=%wide.region_3.4_spmd.clone.sunk | while | flops 41287 | bytes 362514 | solution.py:53
  75.6 5.8 %while.43 = (s32[]{:T(128)}, f32[1,128,64]{2,1,0:T(8,128)S(1)}, f32[1,64]{1,0:T(1,128)S(1)}, f32[1]{0:T(128)}, f32[2,1,128,64]{3,2,1,0:T(8,128)S(1)}, /*index=5*...) while((s32[]{:T(128)}, f32[1,128,64]{2,1,0:T(8,128)S(1)}, ...), condition=%wide.region_11.12_spmd.clone, body=%wide.region_10.11_spmd.clone.sunk | while | flops 41287 | bytes 362514 | solution.py:53
  81.8 2.4 fusion.99
  85.3 3.5 %fusion.18 = f32[2,512,128]{2,1,0:T(8,128)S(1)} fusion(f32[2,512,128]{2,1,0:T(8,128)S(1)} %convolution_multiply_fusion.1, f32[2,512,512]{1,2,0:T(8,128)S(1)} %get-tuple-element.446, f32[2,512,128]{2,1,0:T(8,128)S(1)} %bitcast.339, f32[2,512]{1,0:T(2,128)S(1)} %get-tuple-element.429), kind=kOutput, calls=%fused_computation.41 | convolution fusion | flops 805568512 | bytes 3674112 | tf_op jit(solution)/shard_map/vmap(cts,csv->ctv)/dot_general | solution.py:81
  89.6 1.5 fusion.100
  92.2 1.9 fusion.19
  95.0 2.2 reduce.41
  98.1 3.8 %all-to-all-start.4 = ((bf16[8,2,8192]{2,1,0:T(2,128)(2,1)}), bf16[8,2,8192]{2,1,0:T(2,128)(2,1)S(1)}, u32[]{:S(2)}, u32[]{:S(2)}) async-start(bf16[8,2,8192]{2,1,0:T(2,128)(2,1)} %reshape.1272), calls=%async_computation.4 | async-start | bytes 524288 | tf_op jit(solution)/shard_map/all_to_all | solution.py:169
  102.3 7.7 %all-to-all-done.4 = bf16[8,2,8192]{2,1,0:T(2,128)(2,1)S(1)} async-done(((bf16[8,2,8192]{2,1,0:T(2,128)(2,1)}), bf16[8,2,8192]{2,1,0:T(2,128)(2,1)S(1)}, u32[]{:S(2)}, u32[]{:S(2)}) %all-to-all-start.4) | async-done | bytes 262176 | tf_op jit(solution)/shard_map/all_to_all | solution.py:169
  110.9 3.1 %multiply_reduce_fusion = (f32[128]{0:T(128)S(1)}, f32[128,2048]{1,0:T(8,128)S(1)}) fusion(bf16[1024,2048]{1,0:T(8,128)(2,1)} %all-gather.2.cloned.1.call-done, bf16[1,128,1024]{2,1,0:T(8,128)(2,1)S(1)} %copy-done.11, f32[1,8,16,8,128]{4,3,2,1,0:T(8,128)S(1)} %bitcast.370), kind=kOutput, calls=%fused_computation.54 | convolution fusion | flops 538181504 | bytes 6029824 | tf_op jit(solution)/shard_map/dot_general | solution.py:176
  115.5 51.4 %all_to_all.84 = bf16[32,16,2048]{2,1,0:T(8,128)(2,1)S(1)} all-to-all(bf16[32,16,2048]{2,1,0:T(8,128)(2,1)S(1)} %bitcast.335), channel_id=1, replica_groups=mesh['sp'=8,'dp'=4] {'sp','dp'}, dimensions={0} | all-to-all | bytes 4194304 | tf_op jit(solution)/shard_map/all_to_all | solution.py:207
  166.9 3.7 %fusion.10 = f32[512,1024]{1,0:T(8,128)} fusion(bf16[512,2048]{1,0:T(8,128)(2,1)S(1)} %bitcast.353, bf16[1,2048,1024]{2,1,0:T(8,128)(2,1)S(1)} %copy-done.10), kind=kOutput, calls=%fused_computation.26 | convolution fusion | flops 2147483648 | bytes 8388608 | tf_op jit(solution)/shard_map/dot_general | solution.py:209
  170.6 9.9 %fusion.12 = bf16[512,2048]{1,0:T(8,128)(2,1)} fusion(bf16[1,1024,2048]{2,1,0:T(8,128)(2,1)} %param.39, f32[512,1024]{1,0:T(8,128)} %fusion.10, bf16[512,2048]{1,0:T(8,128)(2,1)S(1)} %bitcast.354, bf16[1,2048,1024]{2,1,0:T(8,128)(2,1)} %param.38), kind=kOutput, calls=%fused_computation.28 | convolution fusion | flops 4299161600 | bytes 14680064 | tf_op jit(solution)/shard_map/dot_general | solution.py:212
  180.5 3.7 %all-to-all-start.6 = ((bf16[32,16,2048]{2,1,0:T(8,128)(2,1)}), bf16[32,16,2048]{2,1,0:T(8,128)(2,1)S(1)}, u32[]{:S(2)}, u32[]{:S(2)}) async-start(bf16[32,16,2048]{2,1,0:T(8,128)(2,1)} %bitcast.352), calls=%async_computation.6 | async-start | bytes 4194304 | tf_op jit(solution)/shard_map/all_to_all | solution.py:215
  184.3 48.6 %all-to-all-done.6 = bf16[32,16,2048]{2,1,0:T(8,128)(2,1)S(1)} async-done(((bf16[32,16,2048]{2,1,0:T(8,128)(2,1)}), bf16[32,16,2048]{2,1,0:T(8,128)(2,1)S(1)}, u32[]{:S(2)}, u32[]{:S(2)}) %all-to-all-start.6) | async-done | bytes 2097184 | tf_op jit(solution)/shard_map/all_to_all | solution.py:215
  (184 shorter events, 39.7 us)
Async XLA Ops:
  6.5 17.2 %copy-start.1 = (bf16[1,128,1024]{2,1,0:T(8,128)(2,1)S(1)}, bf16[1,128,1024]{2,1,0:T(8,128)(2,1)}, u32[]{:S(2)}) copy-start(bf16[1,128,1024]{2,1,0:T(8,128)(2,1)} %param.25) | copy-start | bytes 786436
  9.1 20.6 %all-to-all-start = ((bf16[8,2,256]{2,1,0:T(2,128)(2,1)}), bf16[8,2,256]{2,1,0:T(2,128)(2,1)S(1)}, u32[]{:S(2)}, u32[]{:S(2)}) async-start(bf16[8,2,256]{2,1,0:T(2,128)(2,1)} %reshape.1268), calls=%async_computation | async-start | bytes 16384 | tf_op jit(solution)/shard_map/all_to_all | solution.py:149
  16.4 94.4 %all-gather.2.cloned.1.call-start = ((), (), s32[]{:S(2)}) async-start(), calls=%async_computation.7 | async-start | bytes 5242880 | tf_op jit(solution)/shard_map/all_gather | solution.py:178
  17.2 10.3 %copy-start.2 = (bf16[1,128,512]{2,1,0:T(8,128)(2,1)S(1)}, bf16[1,128,512]{2,1,0:T(8,128)(2,1)}, u32[]{:S(2)}) copy-start(bf16[1,128,512]{2,1,0:T(8,128)(2,1)} %param.23) | copy-start | bytes 393220
  23.0 13.4 %copy-start.3 = (f32[1,1,1024]{2,1,0:T(1,128)S(1)}, f32[1,1,1024]{2,1,0:T(1,128)}, u32[]{:S(2)}) copy-start(f32[1,1,1024]{2,1,0:T(1,128)} %param.28) | copy-start | bytes 12292
  29.8 30.3 %copy-start.6 = (s32[32,3]{0,1:T(4,128)}, s32[32,3]{0,1:T(4,128)S(1)}, u32[]{:S(2)}) copy-start(s32[32,3]{0,1:T(4,128)S(1)} %reduce-window.29) | copy-start | bytes 1156
  29.8 13.3 %all-to-all-start.2 = ((bf16[8,2,4096]{2,1,0:T(2,128)(2,1)}), bf16[8,2,4096]{2,1,0:T(2,128)(2,1)S(1)}, u32[]{:S(2)}, u32[]{:S(2)}) async-start(bf16[8,2,4096]{2,1,0:T(2,128)(2,1)} %reshape.1266), calls=%async_computation.2 | async-start | bytes 262144 | tf_op jit(solution)/shard_map/all_to_all | solution.py:147
  43.1 13.2 %all-to-all-start.3 = ((bf16[8,2,4096]{2,1,0:T(2,128)(2,1)}), bf16[8,2,4096]{2,1,0:T(2,128)(2,1)S(1)}, u32[]{:S(2)}, u32[]{:S(2)}) async-start(bf16[8,2,4096]{2,1,0:T(2,128)(2,1)} %reshape.1270), calls=%async_computation.3 | async-start | bytes 262144 | tf_op jit(solution)/shard_map/all_to_all | solution.py:146
  56.3 11.6 %all-to-all-start.1 = ((bf16[8,2,8192]{2,1,0:T(2,128)(2,1)}), bf16[8,2,8192]{2,1,0:T(2,128)(2,1)S(1)}, u32[]{:S(2)}, u32[]{:S(2)}) async-start(bf16[8,2,8192]{2,1,0:T(2,128)(2,1)} %reshape.1264), calls=%async_computation.1 | async-start | bytes 524288 | tf_op jit(solution)/shard_map/all_to_all | solution.py:148
  92.2 2.1 copy-start.9
  94.4 7.5 %slice-start = ((s32[32,3]{0,1:T(4,128)}), s32[32,2]{0,1:T(2,128)S(1)}, s32[]{:S(2)}) async-start(s32[32,3]{0,1:T(4,128)} %copy-done.6), calls=%async_computation.8 | async-start | bytes 2048 | tf_op jit(solution)/shard_map/slice.5
  95.0 15.9 %copy-start.11 = (bf16[1,128,1024]{2,1,0:T(8,128)(2,1)S(1)}, bf16[1,128,1024]{2,1,0:T(8,128)(2,1)}, u32[]{:S(2)}) copy-start(bf16[1,128,1024]{2,1,0:T(8,128)(2,1)} %param.30) | copy-start | bytes 786436
  98.1 12.0 %all-to-all-start.4 = ((bf16[8,2,8192]{2,1,0:T(2,128)(2,1)}), bf16[8,2,8192]{2,1,0:T(2,128)(2,1)S(1)}, u32[]{:S(2)}, u32[]{:S(2)}) async-start(bf16[8,2,8192]{2,1,0:T(2,128)(2,1)} %reshape.1272), calls=%async_computation.4 | async-start | bytes 524288 | tf_op jit(solution)/shard_map/all_to_all | solution.py:169
  110.9 3.1 %copy-start = (bf16[1,128,2048]{2,1,0:T(8,128)(2,1)S(1)}, bf16[1,128,2048]{2,1,0:T(8,128)(2,1)}, u32[]{:S(2)}) copy-start(bf16[1,128,2048]{2,1,0:T(8,128)(2,1)} %param.22) | copy-start | bytes 1572868
  110.9 3.1 %copy-start.4 = (f32[2048]{0:T(1024)S(1)}, f32[2048]{0:T(1024)}, u32[]{:S(2)}) copy-start(f32[2048]{0:T(1024)} %param.32) | copy-start | bytes 24580
  114.0 0.7 copy-start.5
  115.5 51.4 %copy-start.10 = (bf16[1,2048,1024]{2,1,0:T(8,128)(2,1)S(1)}, bf16[1,2048,1024]{2,1,0:T(8,128)(2,1)}, u32[]{:S(2)}) copy-start(bf16[1,2048,1024]{2,1,0:T(8,128)(2,1)} %param.37) | copy-start | bytes 12582916
  180.5 3.7 %copy-start.7 = (f32[1,128,4]{1,2,0:T(4,128)S(1)}, f32[1,128,4]{1,2,0:T(4,128)}, u32[]{:S(2)}) copy-start(f32[1,128,4]{1,2,0:T(4,128)} %param.35) | copy-start | bytes 6148
  180.5 3.8 %copy-start.8 = (f32[1,128,2]{1,2,0:T(2,128)S(1)}, f32[1,128,2]{1,2,0:T(2,128)}, u32[]{:S(2)}) copy-start(f32[1,128,2]{1,2,0:T(2,128)} %param.36) | copy-start | bytes 3076
  180.5 52.4 %all-to-all-start.6 = ((bf16[32,16,2048]{2,1,0:T(8,128)(2,1)}), bf16[32,16,2048]{2,1,0:T(8,128)(2,1)S(1)}, u32[]{:S(2)}, u32[]{:S(2)}) async-start(bf16[32,16,2048]{2,1,0:T(8,128)(2,1)} %bitcast.352), calls=%async_computation.6 | async-start | bytes 4194304 | tf_op jit(solution)/shard_map/all_to_all | solution.py:215
Sparse Core Ops, SparseCore 0:
  18.8 35.8 all-gather.1
where the time goes:
time: 242 us; the launch traced here: 241 us
  waiting for transfers between devices  65.1 us (27%)
  blocking collectives  51.4 us (21%)
  matrix products  31.7 us (13%)
  starting transfers between devices  30.2 us (12%)
  local copies, waits for them, and re-layouts  22.6 us (9%)
  other arithmetic  18.3 us (8%)
  between operations  14.1 us (6%)
  loops' own time  8.17 us (3%)
    all_to_all x1, blocking collectives, on_device(): lax.all_to_all(outgoing, ('sp', 'dp'), split_axis=0, concat_axis=0, tiled...  51.4 us
    all_to_all x1, waiting for transfers between devices, on_device(): lax.all_to_all(produced, ('sp', 'dp'), split_axis=0, concat_axis=0, tiled...  48.6 us
    dot_general x1, matrix products, on_device(): jnp.dot(hidden, down_weight[0], preferred_element_type=jnp.float32)  9.9 us
    unnamed x44, local copies, waits for them, and re-layouts  8.53 us
    another operation x2, loops' own time, block_states(): lax.scan(advance, initial, (block_end, local_top, local_memory, local_nor...  8.17 us
    unnamed x9, other arithmetic  7.9 us
    all_to_all x1, waiting for transfers between devices, on_device(): lax.all_to_all(mixed_local, 'sp', split_axis=1, concat_axis=2, tiled=True)  7.72 us
    all_to_all x1, starting transfers between devices, on_device(): lax.all_to_all(gate_logits, 'sp', split_axis=2, concat_axis=1, tiled=True)  7.31 us
  transfers between devices with their start and end apart: 7, of which 5 were waited for; matrix products, arithmetic and copies ran while one was open for 21% of the time, Pallas kernels for 0%

commit v1 on v0

v1 whole, which is shorter than its diff:
```python
from functools import partial

import jax
import jax.numpy as jnp
from jax import lax
from jax.experimental import pallas as pl
from jax.experimental.pallas import tpu as pltpu
from jax.sharding import PartitionSpec as P

EPS = 1e-06
MESH = pl.DeviceIdType.MESH
GATE_ROWS = 16


def log_sigmoid(x):
    return jnp.minimum(x, 0.0) - jnp.log1p(jnp.exp(-jnp.abs(x)))


def front_kernel(
    q_ref, k_ref, v_ref, g_ref, offset_ref, extra_ref, amp_ref, logits_ref, w_ref,
    res_ref, cell_gain_ref, expert_gain_ref,
    stream_ref, moe_ref,
    send, recv, gates_t, cols, mixed, mrecv, wfull, proj,
    send_sem, recv_sem, msend_sem, mrecv_sem, wx_send, wx_recv, wc_send, wc_recv, wl_sem,
    *, n, dpn,
):
    tok = q_ref.shape[1]
    dk = q_ref.shape[2] // n
    dv = v_ref.shape[2] // n
    length = n * tok
    wcol = w_ref.shape[1]
    me = lax.axis_index("sp")
    my_dp = lax.axis_index("dp")
    my_x, my_core = my_dp // 2, my_dp % 2
    chips = dpn // 2

    barrier = pltpu.get_barrier_semaphore()

    def greet(sp, dp):
        pl.semaphore_signal(
            barrier, inc=1, device_id={"sp": sp, "dp": dp}, device_id_type=MESH
        )

    for o in range(1, n):
        greet((me + o) % n, my_dp)
    for o in range(1, chips):
        greet(me, ((my_x + o) % chips) * 2 + my_core)
    greet(me, my_x * 2 + 1 - my_core)

    for h in range(n):
        send[h, 0:tok, 0:dk] = k_ref[0, :, h * dk : (h + 1) * dk]
        send[h, 0:tok, dk : 2 * dk] = q_ref[0, :, h * dk : (h + 1) * dk]
        send[h, 0:tok, 2 * dk : 2 * dk + dv] = v_ref[0, :, h * dv : (h + 1) * dv]
    g = g_ref[0].astype(jnp.float32)
    g = jnp.concatenate([g, jnp.zeros((tok, 128 - g.shape[1]), jnp.float32)], axis=1)
    gates_t[...] = g.T
    for h in range(n):
        send[h, tok : tok + GATE_ROWS, 0:tok] = gates_t[4 * h : 4 * h + GATE_ROWS, :].astype(
            jnp.bfloat16
        )
        send[h, tok : tok + GATE_ROWS, tok:] = jnp.zeros(
            (GATE_ROWS, send.shape[2] - tok), jnp.bfloat16
        )

    own_w = pltpu.make_async_copy(w_ref, wfull.at[my_dp], wl_sem)
    own_w.start()

    pl.semaphore_wait(barrier, n - 1 + chips - 1 + 1)

    def qkv_copy(o):
        return pltpu.make_async_remote_copy(
            src_ref=send.at[(me + o) % n],
            dst_ref=recv.at[me],
            send_sem=send_sem.at[o],
            recv_sem=recv_sem.at[o],
            device_id={"sp": (me + o) % n, "dp": my_dp},
            device_id_type=MESH,
        )

    def qkv_arrival(o):
        return pltpu.make_async_remote_copy(
            src_ref=send.at[(me + o) % n],
            dst_ref=recv.at[(me + n - o) % n],
            send_sem=send_sem.at[o],
            recv_sem=recv_sem.at[o],
            device_id={"sp": (me + o) % n, "dp": my_dp},
            device_id_type=MESH,
        )

    def wx_copy(o, slot):
        return pltpu.make_async_remote_copy(
            src_ref=w_ref,
            dst_ref=wfull.at[slot],
            send_sem=wx_send.at[o],
            recv_sem=wx_recv.at[o],
            device_id={"sp": me, "dp": ((my_x + o) % chips) * 2 + my_core},
            device_id_type=MESH,
        )

    def wc_copy(o, src, slot):
        return pltpu.make_async_remote_copy(
            src_ref=src,
            dst_ref=wfull.at[slot],
            send_sem=wc_send.at[o],
            recv_sem=wc_recv.at[o],
            device_id={"sp": me, "dp": my_x * 2 + 1 - my_core},
            device_id_type=MESH,
        )

    for o in range(1, n):
        qkv_copy(o).start()
    for o in range(1, chips):
        wx_copy(o, my_dp).start()
    wc_copy(0, w_ref, my_dp).start()
    recv[me] = send[me]
    for o in range(1, n):
        qkv_arrival(o).wait_recv()

    gates = jnp.concatenate(
        [recv[d, tok : tok + GATE_ROWS, 0:tok].astype(jnp.float32) for d in range(n)], axis=1
    )
    extra = extra_ref[0]
    f = log_sigmoid(gates[1:2] + offset_ref[0:1, 0:1]) + extra
    b = log_sigmoid(gates[3:4] + offset_ref[0:1, 1:2]) + extra
    f = jnp.broadcast_to(f, (8, length))
    b = jnp.broadcast_to(b, (8, length))
    lane = lax.broadcasted_iota(jnp.int32, (8, length), 1)
    step = 1
    while step < length:
        f = f + jnp.where(lane >= step, pltpu.roll(f, step, 1), 0.0)
        b = b + jnp.where(lane < length - step, pltpu.roll(b, length - step, 1), 0.0)
        step *= 2
    row_i = gates[0:1]
    row_f = row_i - f[0:1]
    row_b = gates[2:3] - b[0:1]
    sub = lax.broadcasted_iota(jnp.int32, (128, length), 0)
    stacked = jnp.where(sub == 0, f[0:1], jnp.where(sub == 1, b[0:1], row_i))
    cols[...] = stacked.T

    scale = dk ** (-0.5)
    amp = amp_ref[...]

    def mixed_copy(o, slot):
        return pltpu.make_async_remote_copy(
            src_ref=mixed.at[(me + o) % n],
            dst_ref=mrecv.at[slot],
            send_sem=msend_sem.at[o],
            recv_sem=mrecv_sem.at[o],
            device_id={"sp": (me + o) % n, "dp": my_dp},
            device_id_type=MESH,
        )

    def segment(j, _):
        d = (me + 1 + j) % n
        start = pl.multiple_of(d * tok, tok)
        kq = recv[d, 0:tok, 0 : 2 * dk]
        qs = kq[:, dk:].astype(jnp.float32) * scale
        ks = kq[:, :dk].astype(jnp.float32)
        diag = jnp.sum(qs * ks, axis=1, keepdims=True)
        qs = jnp.concatenate([qs, jnp.zeros_like(qs)], axis=1).astype(jnp.bfloat16)
        kall = recv[:, 0:tok, 0 : 2 * dk].reshape(length, 2 * dk)
        vall = recv[:, 0:tok, 2 * dk : 2 * dk + dv].reshape(length, dv)
        scores = lax.dot_general(
            qs, kall, (((1,), (1,)), ((), ())), preferred_element_type=jnp.float32
        )
        col = cols[pl.ds(start, tok), :]
        col_f, col_b, col_i = col[:, 0:1], col[:, 1:2], col[:, 2:3]
        t_pos = start + lax.broadcasted_iota(jnp.int32, (tok, length), 0)
        s_pos = lax.broadcasted_iota(jnp.int32, (tok, length), 1)
        before = s_pos < t_pos
        weight = scores * jnp.exp(jnp.where(before, col_f + row_f, col_b + row_b))
        diag = diag * jnp.exp(col_i)
        z_f = jnp.sum(jnp.where(before, weight, 0.0), axis=1, keepdims=True) + diag
        z_b = jnp.sum(jnp.where(before, 0.0, weight), axis=1, keepdims=True)
        inv_f = 1.0 / jnp.maximum(jnp.abs(z_f), 1.0)
        inv_b = 1.0 / jnp.maximum(jnp.abs(z_b), 1.0)
        probs = (weight * jnp.where(before, inv_f, inv_b)).astype(jnp.bfloat16)
        total = jnp.dot(probs, vall, preferred_element_type=jnp.float32)
        total = total + (diag * inv_f) * recv[d, 0:tok, 2 * dk : 2 * dk + dv].astype(jnp.float32)
        total = total * lax.rsqrt(jnp.mean(total * total, axis=1, keepdims=True) + EPS) * amp
        mixed[d] = total.astype(jnp.bfloat16)

        @pl.when(j >= 1)
        def _():
            mixed_copy(j, me).start()

        return 0

    lax.fori_loop(0, n, segment, 0)

    for o in range(1, chips):
        wx_copy(o, ((my_x + chips - o) % chips) * 2 + my_core).wait_recv()
        slot = ((my_x + chips - o) % chips) * 2 + my_core
        wc_copy(o, wfull.at[slot], slot).start()
    mrecv[me] = mixed[me]
    sig = jax.nn.sigmoid(logits_ref[0].astype(jnp.float32))
    for o in range(1, n):
        mixed_copy(o, (me + n - o) % n).wait_recv()
    gated = jnp.concatenate([mrecv[h].astype(jnp.float32) for h in range(n)], axis=1) * sig
    gated = gated.astype(jnp.bfloat16)
    own_w.wait()
    partner = 1 - my_core
    wc_copy(0, w_ref, my_x * 2 + partner).wait_recv()
    for o in range(1, chips):
        slot = ((my_x + chips - o) % chips) * 2 + partner
        wc_copy(o, wfull.at[slot], slot).wait_recv()
    for j in range(dpn):
        proj[:, j * wcol : (j + 1) * wcol] = jnp.dot(
            gated, wfull[j], preferred_element_type=jnp.float32
        )
    p = proj[...]
    stream = (
        res_ref[0].astype(jnp.float32)
        + cell_gain_ref[...] * p * lax.rsqrt(jnp.mean(p * p, axis=1, keepdims=True) + EPS)
    ).astype(jnp.bfloat16)
    stream_ref[...] = stream
    s = stream.astype(jnp.float32)
    moe_ref[...] = (
        expert_gain_ref[...] * s * lax.rsqrt(jnp.mean(s * s, axis=1, keepdims=True) + EPS)
    ).astype(jnp.bfloat16)

    for o in range(1, n):
        qkv_copy(o).wait_send()
        mixed_copy(o, me).wait_send()
    for o in range(1, chips):
        wx_copy(o, my_dp).wait_send()
        slot = ((my_x + chips - o) % chips) * 2 + my_core
        wc_copy(o, wfull.at[slot], slot).wait_send()
    wc_copy(0, w_ref, my_dp).wait_send()


def front(
    residual_input, queries, keys, values, gate_logits, retention_offset, log_forget_extra,
    lane_amplifier, output_gate_logits, output_projection, cell_norm_gain, expert_norm_gain,
):
    n, dpn = lax.axis_size("sp"), lax.axis_size("dp")
    tok, width = residual_input.shape[1:]
    dk, dv = queries.shape[2] // n, values.shape[2] // n
    length = n * tok
    dma = pltpu.SemaphoreType.DMA
    vmem = pl.BlockSpec(memory_space=pltpu.VMEM)
    return pl.pallas_call(
        partial(front_kernel, n=n, dpn=dpn),
        out_shape=(
            jax.ShapeDtypeStruct((tok, width), jnp.bfloat16),
            jax.ShapeDtypeStruct((tok, width), jnp.bfloat16),
        ),
        in_specs=[vmem] * 12,
        out_specs=(vmem, vmem),
        scratch_shapes=[
            pltpu.VMEM((n, tok + GATE_ROWS, 2 * dk + dv), jnp.bfloat16),
            pltpu.VMEM((n, tok + GATE_ROWS, 2 * dk + dv), jnp.bfloat16),
            pltpu.VMEM((128, tok), jnp.float32),
            pltpu.VMEM((length, 128), jnp.float32),
            pltpu.VMEM((n, tok, dv), jnp.bfloat16),
            pltpu.VMEM((n, tok, dv), jnp.bfloat16),
            pltpu.VMEM((dpn,) + output_projection.shape, jnp.bfloat16),
            pltpu.VMEM((tok, width), jnp.float32),
            dma((n,)), dma((n,)), dma((n,)), dma((n,)),
            dma((dpn // 2,)), dma((dpn // 2,)), dma((dpn // 2,)), dma((dpn // 2,)),
            dma(()),
        ],
        compiler_params=pltpu.CompilerParams(
            collective_id=0, has_side_effects=True, vmem_limit_bytes=48 * 1024 * 1024
        ),
    )(
        queries, keys, values, gate_logits, retention_offset, log_forget_extra,
        lane_amplifier.reshape(1, dv), output_gate_logits, output_projection,
        residual_input, cell_norm_gain.reshape(1, width), expert_norm_gain.reshape(1, width),
    )


def on_device(
    residual_input,
    queries,
    keys,
    values,
    gate_logits,
    retention_offset,
    log_forget_extra,
    lane_amplifier,
    output_gate_logits,
    output_projection,
    cell_norm_gain,
    expert_norm_gain,
    expert_index,
    group_mixing_weight,
    within_group_weight,
    gate_weight,
    up_weight,
    down_weight,
):
    tok_rows, width = residual_input.shape[1:]
    stream, moe_in = front(
        residual_input, queries, keys, values, gate_logits, retention_offset, log_forget_extra,
        lane_amplifier, output_gate_logits, output_projection, cell_norm_gain, expert_norm_gain,
    )
    stream_f = stream.astype(jnp.float32)
    seq_devices = lax.axis_size("sp")
    seq_groups = lax.axis_size("dp")
    experts = seq_devices * seq_groups
    capacity = 4 * tok_rows // experts
    flat_ids = expert_index.reshape(tok_rows * 2)
    onehot = (flat_ids[:, None] == jnp.arange(experts, dtype=jnp.int32)[None, :]).astype(jnp.int32)
    slot_index = jnp.sum((jnp.cumsum(onehot, axis=0) - onehot) * onehot, axis=1)
    target = flat_ids * capacity + slot_index
    slot_table = (
        target[:, None] == jnp.arange(experts * capacity, dtype=jnp.int32)[None, :]
    ).astype(jnp.bfloat16)
    token_table = jnp.sum(slot_table.reshape(tok_rows, 2, experts * capacity), axis=1)
    outgoing = lax.dot_general(
        token_table, moe_in, (((0,), (0,)), ((), ())), preferred_element_type=jnp.float32
    ).astype(jnp.bfloat16)
    incoming = lax.all_to_all(outgoing, ("sp", "dp"), split_axis=0, concat_axis=0, tiled=True)
    hidden = (
        jax.nn.silu(jnp.dot(incoming, gate_weight[0], preferred_element_type=jnp.float32))
        * jnp.dot(incoming, up_weight[0], preferred_element_type=jnp.float32)
    ).astype(jnp.bfloat16)
    produced = jnp.dot(hidden, down_weight[0], preferred_element_type=jnp.float32).astype(
        jnp.bfloat16
    )
    returned = lax.all_to_all(produced, ("sp", "dp"), split_axis=0, concat_axis=0, tiled=True)
    group_count = group_mixing_weight.shape[2]
    group_of = expert_index.reshape(tok_rows, 2) // (experts // group_count)
    group_hit = (
        group_of[:, :, None] == jnp.arange(group_count, dtype=jnp.int32)[None, None, :]
    ).astype(jnp.float32)
    chosen_group = jnp.sum(
        group_mixing_weight.reshape(tok_rows, 1, group_count) * group_hit, axis=2
    )
    route = chosen_group * within_group_weight.reshape(tok_rows, 2)
    picked = jnp.dot(slot_table, returned, preferred_element_type=jnp.float32).reshape(
        tok_rows, 2, width
    )
    mixture = jnp.sum(picked * route[:, :, None], axis=1)
    return (stream_f + mixture).astype(jnp.bfloat16).reshape(1, tok_rows, width)


def solution(mesh):
    in_specs = (
        P("dp", "sp", None),
        P("dp", "sp", None),
        P("dp", "sp", None),
        P("dp", "sp", None),
        P("dp", "sp", None),
        P("sp", None),
        P("dp", "sp", None),
        P("sp"),
        P("dp", "sp", None),
        P(None, "dp"),
        P(),
        P(),
        P("dp", "sp", None),
        P("dp", "sp", None),
        P("dp", "sp", None),
        P(("sp", "dp"), None, None),
        P(("sp", "dp"), None, None),
        P(("sp", "dp"), None, None),
    )
    out_specs = P("dp", "sp", None)
    return jax.shard_map(
        on_device, mesh=mesh, in_specs=in_specs, out_specs=out_specs, check_vma=False
    )
```

time: 242 us -> 166 us (0.69)
  Pallas kernels: 0 us -> 33.1 us
  starting transfers between devices: 30.2 us -> 3.67 us
  matrix products: 31.7 us -> 15.2 us
  waiting for transfers between devices: 65.1 us -> 48.6 us
  other arithmetic: 18.3 us -> 1.89 us
  between operations: 14.1 us -> 0.12 us
  local copies, waits for them, and re-layouts: 22.6 us -> 11.7 us
  loops' own time: 8.17 us -> 0 us
    pallas_call x0 -> x1, Pallas kernels: none -> 33.1 us  [front(): pl.pallas_call(partial(front_kernel, n=n, dpn=dpn), out_shape=(jax.ShapeD...]
    all_to_all x5 -> x0, starting transfers between devices: 26.5 us -> none  [the longest x1 7.31 us: on_device(): lax.all_to_all(gate_logits, 'sp', split_axis=2, concat_axis=1, tiled=True)]
    dot_general x13 -> x0, matrix products: 16.5 us -> none  [the longest x2 5.43 us: direction_out(): jnp.einsum('cts,csv->ctv', scores, blocked_values, precision=HIGH_PRECISION)]
    all_to_all x5 -> x0, waiting for transfers between devices: 15.7 us -> none  [the longest x1 7.72 us: on_device(): lax.all_to_all(mixed_local, 'sp', split_axis=1, concat_axis=2, tiled=True)]
    another operation x2 -> x0, loops' own time: 8.17 us -> none  [block_states(): lax.scan(advance, initial, (block_end, local_top, local_memory, local_nor...]
    unnamed x9 -> x0, other arithmetic: 7.9 us -> none
    rev x7 -> x0, local copies, waits for them, and re-layouts: 5.94 us -> none  [the longest x1 1.68 us: lane_blend(): keys_f[::-1]]
    dynamic_slice x12 -> x0, local copies, waits for them, and re-layouts: 2.9 us -> none  [block_states(): lax.scan(advance, initial, (block_end, local_top, local_memory, local_nor...]
  transfers between devices with their start and end apart: 7 -> 1, of which waited for: 5 -> 1; matrix products, arithmetic and copies ran while one was open for 21% -> 0% of each run, Pallas kernels for 0% -> 0%
where the time goes in v1:
time: 166 us
  blocking collectives  51.4 us (31%)
  waiting for transfers between devices  48.6 us (29%)
  Pallas kernels  33.1 us (20%)
  matrix products  15.2 us (9%)
  local copies, waits for them, and re-layouts  11.7 us (7%)
  starting transfers between devices  3.67 us (2%)
  other arithmetic  1.89 us (1%)
    all_to_all x1, blocking collectives, on_device(): lax.all_to_all(outgoing, ('sp', 'dp'), split_axis=0, concat_axis=0, tiled...  51.4 us
    all_to_all x1, waiting for transfers between devices, on_device(): lax.all_to_all(produced, ('sp', 'dp'), split_axis=0, concat_axis=0, tiled...  48.6 us
    pallas_call x1, Pallas kernels, front(): pl.pallas_call(partial(front_kernel, n=n, dpn=dpn), out_shape=(jax.ShapeD...  33.1 us
    unnamed x30, local copies, waits for them, and re-layouts  11 us
    dot_general x1, matrix products, on_device(): jnp.dot(hidden, down_weight[0], preferred_element_type=jnp.float32)  9.94 us
    dot_general x1, matrix products, on_device(): jnp.dot(incoming, gate_weight[0], preferred_element_type=jnp.float32)  3.73 us
    all_to_all x1, starting transfers between devices, on_device(): lax.all_to_all(produced, ('sp', 'dp'), split_axis=0, concat_axis=0, tiled...  3.67 us
  transfers between devices with their start and end apart: 1, of which 1 were waited for; matrix products, arithmetic and copies ran while one was open for 0% of the time, Pallas kernels for 0%

profile of v1, /device:TPU:0, one launch (start us, length us, event | category | flops | bytes accessed | tf_op | source)
XLA Modules:
  0.0 165.7 jit_solution(7400718446615587132)
XLA Ops:
  0.0 0.8 copy.31
  1.1 0.8 copy.30.g_ref
  1.9 0.6 reduce-window.6
  2.5 0.2 slice_reduce_fusion
  3.2 1.2 copy-done
  4.5 1.0 copy-done.1
  5.5 0.9 copy-done.2
  6.4 0.9 copy-done.3
  7.4 0.9 copy-done.4
  8.3 0.9 copy-done.5
  9.2 0.7 copy-done.6
  9.9 0.7 copy-done.7
  10.6 0.7 copy-done.8
  11.3 0.7 copy-done.9
  11.9 0.7 copy-done.10
  12.6 33.1 %shard_map.172 = (bf16[128,2048]{1,0:T(8,128)(2,1)S(1)}, bf16[128,2048]{1,0:T(8,128)(2,1)S(1)}) custom-call(bf16[1,128,512]{2,1,0:T(8,128)(2,1)S(1)} %copy-done.4, bf16[1,128,512]{2,1,0:T(8,128)(2,1)S(1)} %copy-done.5, bf16[1,128,1024]{2,1,0:T(8,128)(2,1)S(1)} %copy-done.2, bf16[1,128,32]{2,1,0:T(8,128)(2,1)S(1)} %copy.30.g_ref, f32[1,2]{1,0:T(1,128)S(1)} %copy-done.9, ...), custom_call_target="tpu_custom_call" | custom-call | tf_op jit(solution)/shard_map/pallas_call | solution.py:242
  45.7 0.7 convolution_convert_fusion
  46.4 51.4 %all_to_all.24 = bf16[32,16,2048]{2,1,0:T(8,128)(2,1)S(1)} all-to-all(bf16[32,16,2048]{2,1,0:T(8,128)(2,1)S(1)} %bitcast.78), channel_id=1, replica_groups=mesh['sp'=8,'dp'=4] {'sp','dp'}, dimensions={0} | all-to-all | bytes 4194304 | tf_op jit(solution)/shard_map/all_to_all | solution.py:314
  97.8 3.7 %fusion.4 = f32[512,1024]{1,0:T(8,128)} fusion(bf16[512,2048]{1,0:T(8,128)(2,1)S(1)} %bitcast.81, bf16[1,2048,1024]{2,1,0:T(8,128)(2,1)S(1)} %copy-done.13), kind=kOutput, calls=%fused_computation.4 | convolution fusion | flops 2147483648 | bytes 8388608 | tf_op jit(solution)/shard_map/dot_general | solution.py:316
  101.6 9.9 %fusion.6 = bf16[512,2048]{1,0:T(8,128)(2,1)} fusion(bf16[1,1024,2048]{2,1,0:T(8,128)(2,1)} %param.35, f32[512,1024]{1,0:T(8,128)} %fusion.4, bf16[512,2048]{1,0:T(8,128)(2,1)S(1)} %bitcast.82, bf16[1,2048,1024]{2,1,0:T(8,128)(2,1)} %param.34), kind=kOutput, calls=%fused_computation.6 | convolution fusion | flops 4299161600 | bytes 14680064 | tf_op jit(solution)/shard_map/dot_general | solution.py:319
  111.5 3.7 %all-to-all-start.1 = ((bf16[32,16,2048]{2,1,0:T(8,128)(2,1)}), bf16[32,16,2048]{2,1,0:T(8,128)(2,1)S(1)}, u32[]{:S(2)}, u32[]{:S(2)}) async-start(bf16[32,16,2048]{2,1,0:T(8,128)(2,1)} %bitcast.80), calls=%async_computation.1 | async-start | bytes 4194304 | tf_op jit(solution)/shard_map/all_to_all | solution.py:322
  115.3 48.6 %all-to-all-done.1 = bf16[32,16,2048]{2,1,0:T(8,128)(2,1)S(1)} async-done(((bf16[32,16,2048]{2,1,0:T(8,128)(2,1)}), bf16[32,16,2048]{2,1,0:T(8,128)(2,1)S(1)}, u32[]{:S(2)}, u32[]{:S(2)}) %all-to-all-start.1) | async-done | bytes 2097184 | tf_op jit(solution)/shard_map/all_to_all | solution.py:322
  163.9 0.8 fusion.11
  164.8 0.9 fusion.14
  (30 shorter events, 0.9 us)
Async XLA Ops:
  3.2 1.2 copy-start
  4.5 1.0 copy-start.1
  5.5 0.9 copy-start.2
  6.4 0.9 copy-start.3
  7.4 0.9 copy-start.4
  8.3 0.9 copy-start.5
  9.2 0.7 copy-start.6
  9.9 0.7 copy-start.7
  10.6 0.7 copy-start.8
  11.3 0.7 copy-start.9
  11.9 0.7 copy-start.10
  46.4 51.4 %copy-start.13 = (bf16[1,2048,1024]{2,1,0:T(8,128)(2,1)S(1)}, bf16[1,2048,1024]{2,1,0:T(8,128)(2,1)}, u32[]{:S(2)}) copy-start(bf16[1,2048,1024]{2,1,0:T(8,128)(2,1)} %param.33) | copy-start | bytes 12582916
  111.5 3.7 %copy-start.11 = (f32[1,128,4]{1,2,0:T(4,128)S(1)}, f32[1,128,4]{1,2,0:T(4,128)}, u32[]{:S(2)}) copy-start(f32[1,128,4]{1,2,0:T(4,128)} %param.31) | copy-start | bytes 6148
  111.5 3.8 %copy-start.12 = (f32[1,128,2]{1,2,0:T(2,128)S(1)}, f32[1,128,2]{1,2,0:T(2,128)}, u32[]{:S(2)}) copy-start(f32[1,128,2]{1,2,0:T(2,128)} %param.32) | copy-start | bytes 3076
  111.5 52.4 %all-to-all-start.1 = ((bf16[32,16,2048]{2,1,0:T(8,128)(2,1)}), bf16[32,16,2048]{2,1,0:T(8,128)(2,1)S(1)}, u32[]{:S(2)}, u32[]{:S(2)}) async-start(bf16[32,16,2048]{2,1,0:T(8,128)(2,1)} %bitcast.80), calls=%async_computation.1 | async-start | bytes 4194304 | tf_op jit(solution)/shard_map/all_to_all | solution.py:322

commit v2 on v1

--- a/solution.py
+++ b/solution.py
@@ -10,20 +10,31 @@
 EPS = 1e-06
 MESH = pl.DeviceIdType.MESH
 GATE_ROWS = 16
+CHUNKS = 4
+FF_TILE = 256
 
 
 def log_sigmoid(x):
     return jnp.minimum(x, 0.0) - jnp.log1p(jnp.exp(-jnp.abs(x)))
 
 
-def front_kernel(
-    q_ref, k_ref, v_ref, g_ref, offset_ref, extra_ref, amp_ref, logits_ref, w_ref,
-    res_ref, cell_gain_ref, expert_gain_ref,
-    stream_ref, moe_ref,
-    send, recv, gates_t, cols, mixed, mrecv, wfull, proj,
-    send_sem, recv_sem, msend_sem, mrecv_sem, wx_send, wx_recv, wc_send, wc_recv, wl_sem,
-    *, n, dpn,
-):
+def layer_kernel(*refs, n, dpn, inputs):
+    hbm, (out_ref,), rest = refs[:inputs], refs[inputs : inputs + 1], refs[inputs + 1 :]
+    local, rest = rest[:inputs], rest[inputs:]
+    (
+        q_ref, k_ref, v_ref, g_ref, offset_ref, extra_ref, amp_ref, logits_ref, w_ref,
+        res_ref, cell_gain_ref, expert_gain_ref, index_ref, group_ref, within_ref,
+        gate_ref, up_ref, down_ref,
+    ) = local
+    (
+        send, recv, gates_t, cols, mixed, mrecv, wfull, proj,
+        moe, table_t, table_0, table_1, outgoing, incoming, xs, hs, produced, returned,
+        in_sem, send_sem, recv_sem, msend_sem, mrecv_sem, wx_send, wx_recv, wc_send, wc_recv,
+        wl_sem, out_send, out_recv, back_send, back_recv,
+    ) = rest
+    loads = [pltpu.make_async_copy(hbm[i], local[i], in_sem.at[i]) for i in range(inputs)]
+    for load in loads:
+        load.start()
     tok = q_ref.shape[1]
     dk = q_ref.shape[2] // n
     dv = v_ref.shape[2] // n
@@ -36,16 +47,25 @@
 
     barrier = pltpu.get_barrier_semaphore()
 
-    def greet(sp, dp):
+    devices = n * dpn
+    mine = me * dpn + my_dp
+    cap = 4 * tok // devices
+    per = devices // CHUNKS
+    my_chunk, my_place = mine // per, mine % per
+
+    def greet(o, _):
+        other = (mine + o) % devices
         pl.semaphore_signal(
-            barrier, inc=1, device_id={"sp": sp, "dp": dp}, device_id_type=MESH
-        )
-
-    for o in range(1, n):
-        greet((me + o) % n, my_dp)
-    for o in range(1, chips):
-        greet(me, ((my_x + o) % chips) * 2 + my_core)
-    greet(me, my_x * 2 + 1 - my_core)
+            barrier,
+            inc=1,
+            device_id={"sp": other // dpn, "dp": other % dpn},
+            device_id_type=MESH,
+        )
+        return 0
+
+    lax.fori_loop(1, devices, greet, 0)
+    for load in loads[:4]:
+        load.wait()
 
     for h in range(n):
         send[h, 0:tok, 0:dk] = k_ref[0, :, h * dk : (h + 1) * dk]
@@ -62,10 +82,7 @@
             (GATE_ROWS, send.shape[2] - tok), jnp.bfloat16
         )
 
-    own_w = pltpu.make_async_copy(w_ref, wfull.at[my_dp], wl_sem)
-    own_w.start()
-
-    pl.semaphore_wait(barrier, n - 1 + chips - 1 + 1)
+    pl.semaphore_wait(barrier, devices - 1)
 
     def qkv_copy(o):
         return pltpu.make_async_remote_copy(
@@ -109,10 +126,58 @@
 
     for o in range(1, n):
         qkv_copy(o).start()
+    loads[8].wait()
     for o in range(1, chips):
         wx_copy(o, my_dp).start()
     wc_copy(0, w_ref, my_dp).start()
+    own_w = pltpu.make_async_copy(w_ref, wfull.at[my_dp], wl_sem)
+    own_w.start()
     recv[me] = send[me]
+    for i in (4, 5, 6, 7, 9, 10, 11, 12, 13, 14):
+        loads[i].wait()
+
+    rows_in = per * cap
+    ids = index_ref[0].astype(jnp.float32)
+    e_0, e_1 = ids[:, 0:1], ids[:, 1:2]
+    wide = -(-devices // 128) * 128
+    lane_e = lax.broadcasted_iota(jnp.int32, (tok, wide), 1).astype(jnp.float32)
+    hit_0 = jnp.where(lane_e == e_0, 1.0, 0.0)
+    hit_1 = jnp.where(lane_e == e_1, 1.0, 0.0)
+    tri = jnp.where(
+        lax.broadcasted_iota(jnp.int32, (tok, tok), 1)
+        < lax.broadcasted_iota(jnp.int32, (tok, tok), 0),
+        1.0,
+        0.0,
+    ).astype(jnp.bfloat16)
+    rank_0 = jnp.dot(tri, hit_0.astype(jnp.bfloat16), preferred_element_type=jnp.float32)
+    rank_1 = jnp.dot(tri, hit_1.astype(jnp.bfloat16), preferred_element_type=jnp.float32)
+    rank_1 = rank_1 + jnp.sum(hit_0, axis=0, keepdims=True)
+    place_0 = e_0 * cap + jnp.sum(hit_0 * rank_0, axis=1, keepdims=True)
+    place_1 = e_1 * cap + jnp.sum(hit_1 * rank_1, axis=1, keepdims=True)
+    lane_t = lax.broadcasted_iota(jnp.int32, (tok, tok), 1)
+    turned = jnp.where(lane_t == 0, place_0, place_1).T
+    row_0, row_1 = turned[0:1], turned[1:2]
+    sub_r = lax.broadcasted_iota(jnp.int32, (rows_in, tok), 0).astype(jnp.float32)
+    lane_r = lax.broadcasted_iota(jnp.int32, (tok, rows_in), 1).astype(jnp.float32)
+    for c in range(CHUNKS):
+        at = sub_r + c * rows_in
+        table_t[c] = (jnp.where(at == row_0, 1.0, 0.0) + jnp.where(at == row_1, 1.0, 0.0)).astype(
+            jnp.bfloat16
+        )
+        at = lane_r + c * rows_in
+        table_0[c] = jnp.where(at == place_0, 1.0, 0.0).astype(jnp.bfloat16)
+        table_1[c] = jnp.where(at == place_1, 1.0, 0.0).astype(jnp.bfloat16)
+    groups = group_ref.shape[2]
+    span = devices // groups
+    route_0 = jnp.zeros((tok, 1), jnp.float32)
+    route_1 = jnp.zeros((tok, 1), jnp.float32)
+    for c in range(groups):
+        weight_c = group_ref[0, :, c : c + 1]
+        route_0 += jnp.where((e_0 >= c * span) & (e_0 < (c + 1) * span), weight_c, 0.0)
+        route_1 += jnp.where((e_1 >= c * span) & (e_1 < (c + 1) * span), weight_c, 0.0)
+    route_0 = route_0 * within_ref[0, :, 0:1]
+    route_1 = route_1 * within_ref[0, :, 1:2]
+
     for o in range(1, n):
         qkv_arrival(o).wait_recv()
 
@@ -213,12 +278,128 @@
         res_ref[0].astype(jnp.float32)
         + cell_gain_ref[...] * p * lax.rsqrt(jnp.mean(p * p, axis=1, keepdims=True) + EPS)
     ).astype(jnp.bfloat16)
-    stream_ref[...] = stream
     s = stream.astype(jnp.float32)
-    moe_ref[...] = (
+    proj[...] = s
+    moe[...] = (
         expert_gain_ref[...] * s * lax.rsqrt(jnp.mean(s * s, axis=1, keepdims=True) + EPS)
     ).astype(jnp.bfloat16)
 
+    width = moe.shape[1]
+
+    def copy_of(src, dst, sems, tag, dev, slot_src, slot_dst):
+        return pltpu.make_async_remote_copy(
+            src_ref=src.at[slot_src],
+            dst_ref=dst.at[slot_dst],
+            send_sem=sems[0].at[tag],
+            recv_sem=sems[1].at[tag],
+            device_id={"sp": dev // dpn, "dp": dev % dpn},
+            device_id_type=MESH,
+        )
+
+    def ahead(z, i):
+        return (my_chunk + z) % CHUNKS * per + (my_place + i) % per
+
+    def behind(z, i):
+        return (my_chunk + CHUNKS - z) % CHUNKS * per + (my_place + per - i) % per
+
+    out_sems, back_sems = (out_send, out_recv), (back_send, back_recv)
+
+    def each(z, act):
+        def one(i, _):
+            @pl.when(z * per + i > 0)
+            def _():
+                act(i)
+
+            return 0
+
+        lax.fori_loop(0, per, one, 0)
+
+    def dispatch(z, _):
+        c = (my_chunk + z) % CHUNKS
+        block = jnp.dot(table_t[c], moe[...], preferred_element_type=jnp.float32)
+        outgoing[pl.ds(c * per, per)] = block.astype(jnp.bfloat16).reshape(per, cap, width)
+
+        def start(i):
+            dev = ahead(z, i)
+            copy_of(outgoing, incoming, out_sems, z * per + i, dev, dev, mine).start()
+
+        each(z, start)
+        return 0
+
+    lax.fori_loop(0, CHUNKS, dispatch, 0)
+    incoming[mine] = outgoing[mine]
+    for i in (15, 16, 17):
+        loads[i].wait()
+    ff = hs.shape[1]
+
+    def expert(z, _):
+        c = (my_chunk + CHUNKS - z) % CHUNKS
+
+        def arrive(i):
+            dev = behind(z, i)
+            copy_of(outgoing, incoming, out_sems, z * per + i, dev, dev, dev).wait_recv()
+
+        each(z, arrive)
+        xs[...] = incoming[pl.ds(c * per, per)].reshape(rows_in, width)
+
+        def up_tile(t, _):
+            at = pl.ds(pl.multiple_of(t * FF_TILE, FF_TILE), FF_TILE)
+            x = xs[...]
+            a = jnp.dot(x, gate_ref[0, :, at], preferred_element_type=jnp.float32)
+            u = jnp.dot(x, up_ref[0, :, at], preferred_element_type=jnp.float32)
+            hs[:, at] = (jax.nn.silu(a) * u).astype(jnp.bfloat16)
+            return 0
+
+        lax.fori_loop(0, ff // FF_TILE, up_tile, 0)
+
+        def down_tile(t, _):
+            at = pl.ds(pl.multiple_of(t * FF_TILE, FF_TILE), FF_TILE)
+            y = jnp.dot(hs[...], down_ref[0, :, at], preferred_element_type=jnp.float32)
+            produced[pl.ds(c * per, per), :, at] = y.astype(jnp.bfloat16).reshape(
+                per, cap, FF_TILE
+            )
+            return 0
+
+        lax.fori_loop(0, width // FF_TILE, down_tile, 0)
+
+        def start(i):
+            dev = behind(z, i)
+            copy_of(produced, returned, back_sems, z * per + i, dev, dev, mine).start()
+
+        each(z, start)
+        return 0
+
+    lax.fori_loop(0, CHUNKS, expert, 0)
+    returned[mine] = produced[mine]
+
+    def combine(z, _):
+        c = (my_chunk + z) % CHUNKS
+
+        def arrive(i):
+            dev = ahead(z, i)
+            copy_of(produced, returned, back_sems, z * per + i, dev, dev, dev).wait_recv()
+
+        each(z, arrive)
+        block = returned[pl.ds(c * per, per)].reshape(rows_in, width)
+        proj[...] += route_0 * jnp.dot(
+            table_0[c], block, preferred_element_type=jnp.float32
+        ) + route_1 * jnp.dot(table_1[c], block, preferred_element_type=jnp.float32)
+        return 0
+
+    lax.fori_loop(0, CHUNKS, combine, 0)
+    out_ref[0] = proj[...].astype(jnp.bfloat16)
+
+    def drain(z, _):
+        def left(i):
+            dev = ahead(z, i)
+            copy_of(outgoing, incoming, out_sems, z * per + i, dev, dev, mine).wait_send()
+            dev = behind(z, i)
+            copy_of(produced, returned, back_sems, z * per + i, dev, dev, mine).wait_send()
+
+        each(z, left)
+        return 0
+
+    lax.fori_loop(0, CHUNKS, drain, 0)
     for o in range(1, n):
         qkv_copy(o).wait_send()
         mixed_copy(o, me).wait_send()
@@ -227,47 +408,6 @@
         slot = ((my_x + chips - o) % chips) * 2 + my_core
         wc_copy(o, wfull.at[slot], slot).wait_send()
     wc_copy(0, w_ref, my_dp).wait_send()
-
-
-def front(
-    residual_input, queries, keys, values, gate_logits, retention_offset, log_forget_extra,
-    lane_amplifier, output_gate_logits, output_projection, cell_norm_gain, expert_norm_gain,
-):
-    n, dpn = lax.axis_size("sp"), lax.axis_size("dp")
-    tok, width = residual_input.shape[1:]
-    dk, dv = queries.shape[2] // n, values.shape[2] // n
-    length = n * tok
-    dma = pltpu.SemaphoreType.DMA
-    vmem = pl.BlockSpec(memory_space=pltpu.VMEM)
-    return pl.pallas_call(
-        partial(front_kernel, n=n, dpn=dpn),
-        out_shape=(
-            jax.ShapeDtypeStruct((tok, width), jnp.bfloat16),
-            jax.ShapeDtypeStruct((tok, width), jnp.bfloat16),
-        ),
-        in_specs=[vmem] * 12,
-        out_specs=(vmem, vmem),
-        scratch_shapes=[
-            pltpu.VMEM((n, tok + GATE_ROWS, 2 * dk + dv), jnp.bfloat16),
-            pltpu.VMEM((n, tok + GATE_ROWS, 2 * dk + dv), jnp.bfloat16),
-            pltpu.VMEM((128, tok), jnp.float32),
-            pltpu.VMEM((length, 128), jnp.float32),
-            pltpu.VMEM((n, tok, dv), jnp.bfloat16),
-            pltpu.VMEM((n, tok, dv), jnp.bfloat16),
-            pltpu.VMEM((dpn,) + output_projection.shape, jnp.bfloat16),
-            pltpu.VMEM((tok, width), jnp.float32),
-            dma((n,)), dma((n,)), dma((n,)), dma((n,)),
-            dma((dpn // 2,)), dma((dpn // 2,)), dma((dpn // 2,)), dma((dpn // 2,)),
-            dma(()),
-        ],
-        compiler_params=pltpu.CompilerParams(
-            collective_id=0, has_side_effects=True, vmem_limit_bytes=48 * 1024 * 1024
-        ),
-    )(
-        queries, keys, values, gate_logits, retention_offset, log_forget_extra,
-        lane_amplifier.reshape(1, dv), output_gate_logits, output_projection,
-        residual_input, cell_norm_gain.reshape(1, width), expert_norm_gain.reshape(1, width),
-    )
 
 
 def on_device(
@@ -290,50 +430,57 @@
     up_weight,
     down_weight,
 ):
-    tok_rows, width = residual_input.shape[1:]
-    stream, moe_in = front(
-        residual_input, queries, keys, values, gate_logits, retention_offset, log_forget_extra,
-        lane_amplifier, output_gate_logits, output_projection, cell_norm_gain, expert_norm_gain,
+    n, dpn = lax.axis_size("sp"), lax.axis_size("dp")
+    tok, width = residual_input.shape[1:]
+    dk, dv = queries.shape[2] // n, values.shape[2] // n
+    length, devices, ff = n * tok, n * dpn, gate_weight.shape[2]
+    cap, per = 4 * tok // devices, devices // CHUNKS
+    rows_in = per * cap
+    operands = (
+        queries, keys, values, gate_logits, retention_offset, log_forget_extra,
+        lane_amplifier.reshape(1, dv), output_gate_logits, output_projection,
+        residual_input, cell_norm_gain.reshape(1, width), expert_norm_gain.reshape(1, width),
+        expert_index, group_mixing_weight, within_group_weight,
+        gate_weight, up_weight, down_weight,
     )
-    stream_f = stream.astype(jnp.float32)
-    seq_devices = lax.axis_size("sp")
-    seq_groups = lax.axis_size("dp")
-    experts = seq_devices * seq_groups
-    capacity = 4 * tok_rows // experts
-    flat_ids = expert_index.reshape(tok_rows * 2)
-    onehot = (flat_ids[:, None] == jnp.arange(experts, dtype=jnp.int32)[None, :]).astype(jnp.int32)
-    slot_index = jnp.sum((jnp.cumsum(onehot, axis=0) - onehot) * onehot, axis=1)
-    target = flat_ids * capacity + slot_index
-    slot_table = (
-        target[:, None] == jnp.arange(experts * capacity, dtype=jnp.int32)[None, :]
-    ).astype(jnp.bfloat16)
-    token_table = jnp.sum(slot_table.reshape(tok_rows, 2, experts * capacity), axis=1)
-    outgoing = lax.dot_general(
-        token_table, moe_in, (((0,), (0,)), ((), ())), preferred_element_type=jnp.float32
-    ).astype(jnp.bfloat16)
-    incoming = lax.all_to_all(outgoing, ("sp", "dp"), split_axis=0, concat_axis=0, tiled=True)
-    hidden = (
-        jax.nn.silu(jnp.dot(incoming, gate_weight[0], preferred_element_type=jnp.float32))
-        * jnp.dot(incoming, up_weight[0], preferred_element_type=jnp.float32)
-    ).astype(jnp.bfloat16)
-    produced = jnp.dot(hidden, down_weight[0], preferred_element_type=jnp.float32).astype(
-        jnp.bfloat16
-    )
-    returned = lax.all_to_all(produced, ("sp", "dp"), split_axis=0, concat_axis=0, tiled=True)
-    group_count = group_mixing_weight.shape[2]
-    group_of = expert_index.reshape(tok_rows, 2) // (experts // group_count)
-    group_hit = (
-        group_of[:, :, None] == jnp.arange(group_count, dtype=jnp.int32)[None, None, :]
-    ).astype(jnp.float32)
-    chosen_group = jnp.sum(
-        group_mixing_weight.reshape(tok_rows, 1, group_count) * group_hit, axis=2
-    )
-    route = chosen_group * within_group_weight.reshape(tok_rows, 2)
-    picked = jnp.dot(slot_table, returned, preferred_element_type=jnp.float32).reshape(
-        tok_rows, 2, width
-    )
-    mixture = jnp.sum(picked * route[:, :, None], axis=1)
-    return (stream_f + mixture).astype(jnp.bfloat16).reshape(1, tok_rows, width)
+    dma = pltpu.SemaphoreType.DMA
+    bf16, f32 = jnp.bfloat16, jnp.float32
+    hbm = pl.BlockSpec(memory_space=pltpu.HBM)
+    return pl.pallas_call(
+        partial(layer_kernel, n=n, dpn=dpn, inputs=len(operands)),
+        out_shape=jax.ShapeDtypeStruct((1, tok, width), bf16),
+        in_specs=[hbm] * len(operands),
+        out_specs=pl.BlockSpec(memory_space=pltpu.VMEM),
+        scratch_shapes=[pltpu.VMEM(x.shape, x.dtype) for x in operands]
+        + [
+            pltpu.VMEM((n, tok + GATE_ROWS, 2 * dk + dv), bf16),
+            pltpu.VMEM((n, tok + GATE_ROWS, 2 * dk + dv), bf16),
+            pltpu.VMEM((128, tok), f32),
+            pltpu.VMEM((length, 128), f32),
+            pltpu.VMEM((n, tok, dv), bf16),
+            pltpu.VMEM((n, tok, dv), bf16),
+            pltpu.VMEM((dpn,) + output_projection.shape, bf16),
+            pltpu.VMEM((tok, width), f32),
+            pltpu.VMEM((tok, width), bf16),
+            pltpu.VMEM((CHUNKS, rows_in, tok), bf16),
+            pltpu.VMEM((CHUNKS, tok, rows_in), bf16),
+            pltpu.VMEM((CHUNKS, tok, rows_in), bf16),
+            pltpu.VMEM((devices, cap, width), bf16),
+            pltpu.VMEM((devices, cap, width), bf16),
+            pltpu.VMEM((rows_in, width), bf16),
+            pltpu.VMEM((rows_in, ff), bf16),
+            pltpu.VMEM((devices, cap, width), bf16),
+            pltpu.VMEM((devices, cap, width), bf16),
+            dma((len(operands),)),
+            dma((n,)), dma((n,)), dma((n,)), dma((n,)),
+            dma((dpn // 2,)), dma((dpn // 2,)), dma((dpn // 2,)), dma((dpn // 2,)),
+            dma(()),
+            dma((devices,)), dma((devices,)), dma((devices,)), dma((devices,)),
+        ],
+        compiler_params=pltpu.CompilerParams(
+            collective_id=0, has_side_effects=True, vmem_limit_bytes=60 * 1024 * 1024
+        ),
+    )(*operands)
 
 
 def solution(mesh):

time: 166 us -> 148 us (0.89)
  Pallas kernels: 33.1 us -> 141 us
  blocking collectives: 51.4 us -> 0 us
  waiting for transfers between devices: 48.6 us -> 0 us
  matrix products: 15.2 us -> 0 us
  local copies, waits for them, and re-layouts: 11.7 us -> 7.5 us
  starting transfers between devices: 3.67 us -> 0 us
  other arithmetic: 1.89 us -> 0 us
    pallas_call x1, Pallas kernels: 33.1 us -> 141 us  [on_device(): pl.pallas_call(partial(layer_kernel, n=n, dpn=dpn, inputs=len(operands)),...]
    all_to_all x1 -> x0, blocking collectives: 51.4 us -> none  [on_device(): lax.all_to_all(outgoing, ('sp', 'dp'), split_axis=0, concat_axis=0, tiled...]
    all_to_all x1 -> x0, waiting for transfers between devices: 48.6 us -> none  [on_device(): lax.all_to_all(produced, ('sp', 'dp'), split_axis=0, concat_axis=0, tiled...]
    dot_general x4 -> x0, matrix products: 15.2 us -> none  [the longest x1 9.94 us: on_device(): jnp.dot(hidden, down_weight[0], preferred_element_type=jnp.float32)]
    all_to_all x1 -> x0, starting transfers between devices: 3.67 us -> none  [on_device(): lax.all_to_all(produced, ('sp', 'dp'), split_axis=0, concat_axis=0, tiled...]
    unnamed x30 -> x5, local copies, waits for them, and re-layouts: 11 us -> 7.5 us
  transfers between devices with their start and end apart: 1 -> 0, of which waited for: 1 -> 0; matrix products, arithmetic and copies ran while one was open for 0% -> 0% of each run, Pallas kernels for 0% -> 0%
where the time goes in v2:
time: 148 us
  Pallas kernels  141 us (95%)
  local copies, waits for them, and re-layouts  7.5 us (5%)
    pallas_call x1, Pallas kernels, on_device(): pl.pallas_call(partial(layer_kernel, n=n, dpn=dpn, inputs=len(operands)),...  141 us
    unnamed x5, local copies, waits for them, and re-layouts  7.5 us

profile of v2, /device:TPU:0, one launch (start us, length us, event | category | flops | bytes accessed | tf_op | source)
XLA Modules:
  0.0 148.1 jit_solution(18133468415732571256)
XLA Ops:
  0.0 1.4 copy.19.refs_3_
  1.4 1.4 copy.20.refs_12_
  2.8 1.4 copy.21.refs_13_
  4.2 1.4 copy.22.refs_14_
  5.6 140.5 %shard_map.172 = bf16[1,128,2048]{2,1,0:T(8,128)(2,1)} custom-call(bf16[1,128,512]{2,1,0:T(8,128)(2,1)} %refs_0_.1, bf16[1,128,512]{2,1,0:T(8,128)(2,1)} %refs_1_.1, bf16[1,128,1024]{2,1,0:T(8,128)(2,1)} %refs_2_.1, bf16[1,128,32]{2,1,0:T(8,128)(2,1)} %copy.19.refs_3_, f32[1,2]{1,0:T(1,128)} %refs_4_.1, f32[1,1,1024]{2,1,0:T(1,128)} %refs_5_.1, ...), custom_call_target="tpu_custom_call" | custom-call | tf_op jit(solution)/shard_map/pallas_call | solution.py:449
  146.2 1.9 %copy.24 = bf16[1,128,2048]{2,1,0:T(8,128)(2,1)} copy(bf16[1,128,2048]{2,1,0:T(8,128)(2,1)} %shard_map.172) | data formatting | bytes 1048576

commit v3 on v2

--- a/solution.py
+++ b/solution.py
@@ -12,6 +12,7 @@
 GATE_ROWS = 16
 CHUNKS = 4
 FF_TILE = 256
+PIECES = 4
 
 
 def log_sigmoid(x):
@@ -104,32 +105,44 @@
             device_id_type=MESH,
         )
 
-    def wx_copy(o, slot):
+    piece = w_ref.shape[0] // PIECES
+
+    def wx_copy(o, p, slot):
         return pltpu.make_async_remote_copy(
-            src_ref=w_ref,
-            dst_ref=wfull.at[slot],
-            send_sem=wx_send.at[o],
-            recv_sem=wx_recv.at[o],
+            src_ref=w_ref.at[pl.ds(p * piece, piece)],
+            dst_ref=wfull.at[slot, pl.ds(p * piece, piece)],
+            send_sem=wx_send.at[o, p],
+            recv_sem=wx_recv.at[o, p],
             device_id={"sp": me, "dp": ((my_x + o) % chips) * 2 + my_core},
             device_id_type=MESH,
         )
 
-    def wc_copy(o, src, slot):
+    def wc_copy(o, p, src, slot):
         return pltpu.make_async_remote_copy(
-            src_ref=src,
-            dst_ref=wfull.at[slot],
-            send_sem=wc_send.at[o],
-            recv_sem=wc_recv.at[o],
+            src_ref=src.at[pl.ds(p * piece, piece)],
+            dst_ref=wfull.at[slot, pl.ds(p * piece, piece)],
+            send_sem=wc_send.at[o, p],
+            recv_sem=wc_recv.at[o, p],
             device_id={"sp": me, "dp": my_x * 2 + 1 - my_core},
             device_id_type=MESH,
         )
+
+    def from_chip(o):
+        return ((my_x + chips - o) % chips) * 2 + my_core
+
+    def pass_on(p):
+        for o in range(1, chips):
+            slot = from_chip(o)
+            wx_copy(o, p, slot).wait_recv()
+            wc_copy(o, p, wfull.at[slot], slot).start()
 
     for o in range(1, n):
         qkv_copy(o).start()
     loads[8].wait()
-    for o in range(1, chips):
-        wx_copy(o, my_dp).start()
-    wc_copy(0, w_ref, my_dp).start()
+    for p in range(PIECES):
+        for o in range(1, chips):
+            wx_copy(o, p, my_dp).start()
+        wc_copy(0, p, w_ref, my_dp).start()
     own_w = pltpu.make_async_copy(w_ref, wfull.at[my_dp], wl_sem)
     own_w.start()
     recv[me] = send[me]
@@ -249,14 +262,16 @@
         def _():
             mixed_copy(j, me).start()
 
+        @pl.when(j == n // 2)
+        def _():
+            pass_on(PIECES - 2)
+
         return 0
 
+    for p in range(PIECES - 2):
+        pass_on(p)
     lax.fori_loop(0, n, segment, 0)
-
-    for o in range(1, chips):
-        wx_copy(o, ((my_x + chips - o) % chips) * 2 + my_core).wait_recv()
-        slot = ((my_x + chips - o) % chips) * 2 + my_core
-        wc_copy(o, wfull.at[slot], slot).start()
+    pass_on(PIECES - 1)
     mrecv[me] = mixed[me]
     sig = jax.nn.sigmoid(logits_ref[0].astype(jnp.float32))
     for o in range(1, n):
@@ -265,10 +280,11 @@
     gated = gated.astype(jnp.bfloat16)
     own_w.wait()
     partner = 1 - my_core
-    wc_copy(0, w_ref, my_x * 2 + partner).wait_recv()
-    for o in range(1, chips):
-        slot = ((my_x + chips - o) % chips) * 2 + partner
-        wc_copy(o, wfull.at[slot], slot).wait_recv()
+    for p in range(PIECES):
+        wc_copy(0, p, w_ref, my_x * 2 + partner).wait_recv()
+        for o in range(1, chips):
+            slot = ((my_x + chips - o) % chips) * 2 + partner
+            wc_copy(o, p, wfull.at[slot], slot).wait_recv()
     for j in range(dpn):
         proj[:, j * wcol : (j + 1) * wcol] = jnp.dot(
             gated, wfull[j], preferred_element_type=jnp.float32
@@ -314,7 +330,8 @@
 
         lax.fori_loop(0, per, one, 0)
 
-    def dispatch(z, _):
+    def dispatch(turn, _):
+        z = (turn + 1) % CHUNKS
         c = (my_chunk + z) % CHUNKS
         block = jnp.dot(table_t[c], moe[...], preferred_element_type=jnp.float32)
         outgoing[pl.ds(c * per, per)] = block.astype(jnp.bfloat16).reshape(per, cap, width)
@@ -332,7 +349,8 @@
         loads[i].wait()
     ff = hs.shape[1]
 
-    def expert(z, _):
+    def expert(turn, _):
+        z = (turn + 1) % CHUNKS
         c = (my_chunk + CHUNKS - z) % CHUNKS
 
         def arrive(i):
@@ -372,7 +390,8 @@
     lax.fori_loop(0, CHUNKS, expert, 0)
     returned[mine] = produced[mine]
 
-    def combine(z, _):
+    def combine(turn, _):
+        z = (turn + 1) % CHUNKS
         c = (my_chunk + z) % CHUNKS
 
         def arrive(i):
@@ -403,11 +422,12 @@
     for o in range(1, n):
         qkv_copy(o).wait_send()
         mixed_copy(o, me).wait_send()
-    for o in range(1, chips):
-        wx_copy(o, my_dp).wait_send()
-        slot = ((my_x + chips - o) % chips) * 2 + my_core
-        wc_copy(o, wfull.at[slot], slot).wait_send()
-    wc_copy(0, w_ref, my_dp).wait_send()
+    for p in range(PIECES):
+        for o in range(1, chips):
+            wx_copy(o, p, my_dp).wait_send()
+            slot = from_chip(o)
+            wc_copy(o, p, wfull.at[slot], slot).wait_send()
+        wc_copy(0, p, w_ref, my_dp).wait_send()
 
 
 def on_device(
@@ -473,7 +493,8 @@
             pltpu.VMEM((devices, cap, width), bf16),
             dma((len(operands),)),
             dma((n,)), dma((n,)), dma((n,)), dma((n,)),
-            dma((dpn // 2,)), dma((dpn // 2,)), dma((dpn // 2,)), dma((dpn // 2,)),
+            dma((dpn // 2, PIECES)), dma((dpn // 2, PIECES)),
+            dma((dpn // 2, PIECES)), dma((dpn // 2, PIECES)),
             dma(()),
             dma((devices,)), dma((devices,)), dma((devices,)), dma((devices,)),
         ],

time: 148 us -> 147 us (level)
  Pallas kernels: 141 us -> 139 us
    pallas_call x1, Pallas kernels: 141 us -> 139 us  [on_device(): pl.pallas_call(partial(layer_kernel, n=n, dpn=dpn, inputs=len(operands)),...]
where the time goes in v3:
time: 147 us; the launch traced here: 146 us
  Pallas kernels  139 us (95%)
  local copies, waits for them, and re-layouts  7.5 us (5%)
    pallas_call x1, Pallas kernels, on_device(): pl.pallas_call(partial(layer_kernel, n=n, dpn=dpn, inputs=len(operands)),...  139 us
    unnamed x5, local copies, waits for them, and re-layouts  7.5 us

profile of v3, /device:TPU:0, one launch (start us, length us, event | category | flops | bytes accessed | tf_op | source)
XLA Modules:
  0.0 146.4 jit_solution(17075006269301743969)
XLA Ops:
  0.0 1.4 copy.19.refs_3_
  1.4 1.4 copy.20.refs_12_
  2.8 1.4 copy.21.refs_13_
  4.2 1.4 copy.22.refs_14_
  5.6 138.9 %shard_map.172 = bf16[1,128,2048]{2,1,0:T(8,128)(2,1)} custom-call(bf16[1,128,512]{2,1,0:T(8,128)(2,1)} %refs_0_.1, bf16[1,128,512]{2,1,0:T(8,128)(2,1)} %refs_1_.1, bf16[1,128,1024]{2,1,0:T(8,128)(2,1)} %refs_2_.1, bf16[1,128,32]{2,1,0:T(8,128)(2,1)} %copy.19.refs_3_, f32[1,2]{1,0:T(1,128)} %refs_4_.1, f32[1,1,1024]{2,1,0:T(1,128)} %refs_5_.1, ...), custom_call_target="tpu_custom_call" | custom-call | tf_op jit(solution)/shard_map/pallas_call | solution.py:469
  144.6 1.9 %copy.24 = bf16[1,128,2048]{2,1,0:T(8,128)(2,1)} copy(bf16[1,128,2048]{2,1,0:T(8,128)(2,1)} %shard_map.172) | data formatting | bytes 1048576
